TPU v7x, 32 devices: a whole 2x2x4 slice. The times are simulated.
32 devices in a mesh: grp: 2 (over y), sp: 4 (over z), tp: 4 (over x, core).
Axes of the slice: x: 2, y: 2, z: 4, core: 2. Of those that a mesh axis runs over, the one named last changes fastest.
Arguments:
- tokens: bfloat16 [2048, 4096], P(('grp', 'sp')), parts along dimension 0, may hold values from -6 to 6
- norm_gain: bfloat16 [2, 4096], replicated, may hold values from 0.099609375 to 1.8984375
- w_query: bfloat16 [2, 4096, 2048], P(None, 'sp', 'tp'), may hold values from -0.09375 to 0.09375
- w_key: bfloat16 [2, 4096, 2048], P(None, 'sp', 'tp'), may hold values from -0.09375 to 0.09375
- w_value: bfloat16 [2, 4096, 2048], P(None, 'sp', 'tp'), may hold values from -0.09375 to 0.09375
- w_out: bfloat16 [2, 2048, 4096], P(None, 'tp', 'sp'), may hold values from -0.125 to 0.125
- offset_bias: float32 [2, 16, 15, 31], P(None, 'tp'), may hold values from -4 to 300
Outputs:
- mixed: bfloat16 [2048, 4096], P(('grp', 'sp')), parts along dimension 0
There are 2 independent parts, one for each index of `grp`. A program takes and returns all parts, laid end to end along the dimension named above; an argument that names none is the same for every part. Nothing has to cross between parts.
All inputs are finite; a program needn't handle non-finite values.
Results may differ from a plain program's by a relative error of at most 0.013.
Values may be sent and summed in bfloat16 or wider, within the bound.
No kernel may reach another device: no remote copies, remote signals or barrier semaphores. Data moves between devices by JAX's collectives and lax.ppermute only.
A program may use at most 128 MiB of HBM per device.

v0:
```python
import jax
import jax.numpy as jnp
from jax import lax
from jax.sharding import PartitionSpec as P

HD = 128
GRID_W = 64
KR = 8
KC = 16
LAYERS = 2
norm_eps = 1e-06


def with_halo(block, sides, width):
    for axis, dim in sides:
        count = lax.axis_size(axis)
        forward = [(i, i + 1) for i in range(count - 1)]
        backward = [(target, source) for source, target in forward]
        low = lax.ppermute(
            lax.slice_in_dim(block, block.shape[dim] - width, None, axis=dim), axis, forward
        )
        high = lax.ppermute(lax.slice_in_dim(block, 0, width, axis=dim), axis, backward)
        block = jnp.concatenate([low, block, high], axis=dim)
    return block


def rms_rows(values, gain):
    wide = values.astype(jnp.float32)
    scaled = wide * lax.rsqrt(jnp.mean(wide * wide, axis=-1, keepdims=True) + norm_eps)
    return (scaled * gain.astype(jnp.float32)).astype(jnp.bfloat16)


def on_device(tokens, norm_gain, w_query, w_key, w_value, w_out, offset_bias):
    sp_count = lax.axis_size("sp")
    sp_index = lax.axis_index("sp")
    tok_rows = tokens.shape[0]
    local_rows = tok_rows // GRID_W
    grid_rows = local_rows * sp_count
    heads_here = offset_bias.shape[1]
    head_width = heads_here * HD
    reach = KR // 2
    scale = HD ** (-0.5)
    columns = jnp.arange(GRID_W, dtype=jnp.int32)
    col_first = jnp.clip(columns - KC // 2, 0, GRID_W - KC)
    col_inside = (columns[None, :] >= col_first[:, None]) & (
        columns[None, :] < col_first[:, None] + KC
    )
    col_offset = jnp.clip(columns[None, :] - columns[:, None], 1 - KC, KC - 1) + KC - 1
    col_onehot = (
        jnp.arange(2 * KC - 1, dtype=jnp.int32)[:, None, None] == col_offset[None, :, :]
    ).astype(jnp.float32)
    first_row = sp_index * local_rows
    own_rows = first_row + jnp.arange(local_rows, dtype=jnp.int32)
    row_first = jnp.clip(own_rows - reach, 0, grid_rows - KR)
    band_start = row_first - first_row + reach
    row_offset = (
        row_first[:, None] + jnp.arange(KR, dtype=jnp.int32)[None, :] - own_rows[:, None] + KR - 1
    )
    row_onehot = (
        row_offset[:, :, None] == jnp.arange(2 * KR - 1, dtype=jnp.int32)[None, None, :]
    ).astype(jnp.float32)
    every_query, every_key, every_value, every_out = (
        lax.all_gather(w_query, "sp", axis=1, tiled=True),
        lax.all_gather(w_key, "sp", axis=1, tiled=True),
        lax.all_gather(w_value, "sp", axis=1, tiled=True),
        lax.all_gather(w_out, "sp", axis=2, tiled=True),
    )
    residual = tokens
    for layer_index in range(LAYERS):
        normed = rms_rows(residual, norm_gain[layer_index])
        queries = jnp.dot(normed, every_query[layer_index], preferred_element_type=jnp.float32)
        keys = jnp.dot(normed, every_key[layer_index], preferred_element_type=jnp.float32)
        values = jnp.dot(normed, every_value[layer_index], preferred_element_type=jnp.float32)
        out_weight = every_out[layer_index]
        queries = queries.astype(jnp.bfloat16).reshape(local_rows, GRID_W, heads_here, HD)
        key_values = jnp.concatenate(
            [keys.astype(jnp.bfloat16), values.astype(jnp.bfloat16)], axis=1
        )
        key_values = key_values.reshape(local_rows, GRID_W, 2 * head_width)
        padded = with_halo(key_values, (("sp", 0),), reach)
        bands = jax.vmap(lambda band_begin: lax.dynamic_slice_in_dim(padded, band_begin, KR, 0))(
            band_start
        )
        band_keys = bands[..., :head_width].reshape(local_rows, KR, GRID_W, heads_here, HD)
        band_values = bands[..., head_width:].reshape(local_rows, KR, GRID_W, heads_here, HD)
        col_bias = jnp.einsum(
            "hro,oqk->hrqk", offset_bias[layer_index], col_onehot, precision=lax.Precision.HIGHEST
        )
        full_bias = jnp.einsum(
            "ijr,hrqk->hiqjk", row_onehot, col_bias, precision=lax.Precision.HIGHEST
        )
        scores = jnp.einsum(
            "iqhd,ijkhd->hiqjk", queries, band_keys, preferred_element_type=jnp.float32
        )
        scores = scores * scale + full_bias
        scores = jnp.where(col_inside[None, None, :, None, :], scores, -jnp.inf)
        flattened = scores.reshape(heads_here, local_rows, GRID_W, KR * GRID_W)
        weights = jax.nn.softmax(flattened, axis=-1).astype(jnp.bfloat16)
        weights = weights.reshape(heads_here, local_rows, GRID_W, KR, GRID_W)
        attended = jnp.einsum(
            "hiqjk,ijkhd->iqhd", weights, band_values, preferred_element_type=jnp.float32
        )
        attended = attended.astype(jnp.bfloat16).reshape(tok_rows, head_width)
        branch = lax.psum(
            jnp.dot(attended, out_weight, preferred_element_type=jnp.float32).astype(jnp.bfloat16),
            "tp",
        ).astype(jnp.float32)
        residual = (residual.astype(jnp.float32) + branch).astype(jnp.bfloat16)
    return residual


def solution(mesh):
    return jax.shard_map(
        on_device,
        mesh=mesh,
        in_specs=(
            P(("grp", "sp"), None),
            P(),
            P(None, "sp", "tp"),
            P(None, "sp", "tp"),
            P(None, "sp", "tp"),
            P(None, "tp", "sp"),
            P(None, "tp", None, None),
        ),
        out_specs=P(("grp", "sp"), None),
        check_vma=False,
    )
```

profile of v0, /device:TPU:0, one launch (start us, length us, event | category | flops | bytes accessed | tf_op | source)
XLA Modules:
  0.0 783.5 jit_solution(1764364375646308337)
XLA Ops:
  10.7 3.8 fusion.30
  14.5 6.0 copy.16
  21.1 140.2 %all-gather.5.cloned.1.call-done = bf16[2,4096,512]{2,1,0:T(8,128)(2,1)} async-done(((bf16[2,1024,512]{2,1,0:T(8,128)(2,1)}), bf16[2,4096,512]{2,1,0:T(8,128)(2,1)}) %all-gather.5.cloned.1.call-update) | async-done | bytes 8388624 | tf_op jit(solution)/shard_map/all_gather | solution.py:64
  161.3 3.5 fusion.54
  164.7 145.9 %all-gather.7.cloned.1.call-done = bf16[2,4096,512]{2,1,0:T(8,128)(2,1)} async-done(((bf16[2,1024,512]{2,1,0:T(8,128)(2,1)}), bf16[2,4096,512]{2,1,0:T(8,128)(2,1)}) %all-gather.7.cloned.1.call-update) | async-done | bytes 8388624 | tf_op jit(solution)/shard_map/all_gather | solution.py:65
  310.7 3.5 fusion.55
  314.2 2.1 collective-permute-start
  316.3 1.5 collective-permute-start.1
  317.8 149.6 %all-gather.9.cloned.1.call-done = bf16[2,4096,512]{2,1,0:T(8,128)(2,1)} async-done(((bf16[2,1024,512]{2,1,0:T(8,128)(2,1)}), bf16[2,4096,512]{2,1,0:T(8,128)(2,1)}) %all-gather.9.cloned.1.call-update) | async-done | bytes 8388624 | tf_op jit(solution)/shard_map/all_gather | solution.py:63
  467.4 3.5 fusion.56
  471.0 2.5 pad_maximum_fusion
  473.5 4.4 gather_fusion
  477.9 3.5 slice_bitcast_fusion.19
  484.9 132.0 %all-gather.11.cloned.1.call-done = bf16[2,512,4096]{2,1,0:T(8,128)(2,1)} async-done(((bf16[2,512,1024]{2,1,0:T(8,128)(2,1)}), bf16[2,512,4096]{2,1,0:T(8,128)(2,1)}) %all-gather.11.cloned.1.call-update) | async-done | bytes 8388624 | tf_op jit(solution)/shard_map/all_gather | solution.py:66
  616.9 4.8 convolution_convert_fusion.1
  621.8 2.4 fusion.71
  624.2 47.2 %all-reduce.4.cloned.1.call-done = bf16[256,4096]{1,0:T(8,128)(2,1)} async-done(((bf16[256,4096]{1,0:T(8,128)(2,1)}), bf16[256,4096]{1,0:T(8,128)(2,1)}) %all-reduce.4.cloned.1.call-update) | async-done | bytes 2097168 | tf_op jit(solution)/shard_map/psum | solution.py:104
  671.5 2.5 fusion.4
  675.0 4.5 fusion.57
  679.5 1.2 fusion.58
  680.8 3.4 collective-permute-start.2
  684.3 1.5 collective-permute-start.3
  685.8 3.9 fusion.28
  689.7 5.8 copy.22
  695.4 4.8 fusion.59
  701.3 2.4 pad_maximum_fusion.1
  703.6 4.2 gather_fusion.1
  707.8 3.1 slice_bitcast_fusion.17
  714.5 1.5 slice-done.1
  715.9 2.6 convolution_convert_fusion
  718.6 53.4 %all-reduce.6.cloned.1.call-done = bf16[256,4096]{1,0:T(8,128)(2,1)} async-done(((bf16[256,4096]{1,0:T(8,128)(2,1)}), bf16[256,4096]{1,0:T(8,128)(2,1)}) %all-reduce.6.cloned.1.call-update) | async-done | bytes 2097168 | tf_op jit(solution)/shard_map/psum | solution.py:104
  771.9 4.7 fusion.7
  (67 shorter events, 13.9 us)
Async XLA Ops:
  6.5 2.9 copy-start.7
  6.5 154.7 %all-gather.5.cloned.1.call-start = ((), (), s32[]{:S(2)}) async-start(), calls=%async_computation | async-start | bytes 10485760 | tf_op jit(solution)/shard_map/all_gather | solution.py:64
  7.3 303.4 %all-gather.7.cloned.1.call-start = ((), (), s32[]{:S(2)}) async-start(), calls=%async_computation.1 | async-start | bytes 10485760 | tf_op jit(solution)/shard_map/all_gather | solution.py:65
  8.0 459.4 %all-gather.9.cloned.1.call-start = ((), (), s32[]{:S(2)}) async-start(), calls=%async_computation.2 | async-start | bytes 10485760 | tf_op jit(solution)/shard_map/all_gather | solution.py:63
  8.7 608.2 %all-gather.11.cloned.1.call-start = ((), (), s32[]{:S(2)}) async-start(), calls=%async_computation.3 | async-start | bytes 10485760 | tf_op jit(solution)/shard_map/all_gather | solution.py:66
  9.3 662.1 %all-reduce.4.cloned.1.call-start = ((), (), s32[]{:S(2)}) async-start(), calls=%async_computation.4 | async-start | bytes 4194304 | tf_op jit(solution)/shard_map/psum | solution.py:104
  14.5 6.0 copy-start
  14.5 6.6 copy-start.6
  314.2 156.7 %collective-permute-start = (bf16[4,64,1024]{2,1,0:T(8,128)(2,1)S(1)}, bf16[4,64,1024]{2,1,0:T(8,128)(2,1)}, u32[]{:S(2)}, u32[]{:S(2)}) collective-permute-start(bf16[4,64,1024]{2,1,0:T(8,128)(2,1)S(1)} %bitcast.150), channel_id=1, source_target_pairs={{0,4},{4,8},{8,12},{1,5},{5,9},{9,13},{2,6},{6,10},{10,14},{3,7},{... | collective-permute-start | bytes 1572872 | tf_op jit(solution)/shard_map/ppermute | solution.py:19
  316.3 154.6 %collective-permute-start.1 = (bf16[4,64,1024]{2,1,0:T(8,128)(2,1)S(1)}, bf16[4,64,1024]{2,1,0:T(8,128)(2,1)}, u32[]{:S(2)}, u32[]{:S(2)}) collective-permute-start(bf16[4,64,1024]{2,1,0:T(8,128)(2,1)S(1)} %bitcast.151), channel_id=1, source_target_pairs={{4,0},{8,4},{12,8},{5,1},{9,5},{13,9},{6,2},{10,6},{14,10},{7,3},{... | collective-permute-start | bytes 1572872 | tf_op jit(solution)/shard_map/ppermute | solution.py:22
  477.9 4.1 copy-start.2
  621.7 150.2 %all-reduce.6.cloned.1.call-start = ((), (), s32[]{:S(2)}) async-start(), calls=%async_computation.5 | async-start | bytes 4194304 | tf_op jit(solution)/shard_map/psum | solution.py:104
  671.5 2.5 copy-start.1
  674.0 5.5 slice-start.2
  674.9 4.5 copy-start.5
  675.0 4.6 slice-start.3
  679.5 6.3 copy-start.4
  680.8 20.4 %collective-permute-start.2 = (bf16[4,64,1024]{2,1,0:T(8,128)(2,1)S(1)}, bf16[4,64,1024]{2,1,0:T(8,128)(2,1)S(1)}, u32[]{:S(2)}, u32[]{:S(2)}) collective-permute-start(bf16[4,64,1024]{2,1,0:T(8,128)(2,1)S(1)} %bitcast.147), channel_id=1, source_target_pairs={{0,4},{4,8},{8,12},{1,5},{5,9},{9,13},{2,6},{6,10},{10,14},{3,7},{... | collective-permute-start | bytes 1572872 | tf_op jit(solution)/shard_map/ppermute | solution.py:19
  684.3 17.0 %collective-permute-start.3 = (bf16[4,64,1024]{2,1,0:T(8,128)(2,1)S(1)}, bf16[4,64,1024]{2,1,0:T(8,128)(2,1)}, u32[]{:S(2)}, u32[]{:S(2)}) collective-permute-start(bf16[4,64,1024]{2,1,0:T(8,128)(2,1)S(1)} %bitcast.148), channel_id=1, source_target_pairs={{4,0},{8,4},{12,8},{5,1},{9,5},{13,9},{6,2},{10,6},{14,10},{7,3},{... | collective-permute-start | bytes 1572872 | tf_op jit(solution)/shard_map/ppermute | solution.py:22
  707.8 3.4 copy-start.3
  712.3 2.2 slice-start
  713.0 2.9 slice-start.1
Sparse Core Ops, SparseCore 0:
  8.9 152.3 all-gather.4
  162.8 147.7 all-gather.6
  312.2 155.1 all-gather.8
  468.8 148.0 all-gather.10
  621.9 49.5 all-reduce.3
  718.7 53.1 all-reduce.5
where the time goes:
time: 784 us; the launch traced here: 783 us
  waiting for transfers between devices  671 us (86%)
  matrix products  43.4 us (6%)
  local copies, waits for them, and re-layouts  31.2 us (4%)
  other arithmetic  15.4 us (2%)
  between operations  13.8 us (2%)
  starting transfers between devices  8.71 us (1%)
    all_gather x1, waiting for transfers between devices, on_device(): lax.all_gather(w_query, 'sp', axis=1, tiled=True)  150 us
    all_gather x1, waiting for transfers between devices, on_device(): lax.all_gather(w_value, 'sp', axis=1, tiled=True)  146 us
    all_gather x1, waiting for transfers between devices, on_device(): lax.all_gather(w_key, 'sp', axis=1, tiled=True)  140 us
    all_gather x1, waiting for transfers between devices, on_device(): lax.all_gather(w_out, 'sp', axis=2, tiled=True)  132 us
    psum x2, waiting for transfers between devices, on_device(): lax.psum(jnp.dot(attended, out_weight, preferred_element_type=jnp.float32...  101 us
  transfers between devices with their start and end apart: 10, of which 6 were waited for; matrix products, arithmetic and copies ran while one was open for 7% of the time, Pallas kernels for 0%

commit v1 on v0

--- a/solution.py
+++ b/solution.py
@@ -61,7 +61,7 @@
     ).astype(jnp.float32)
     every_query, every_key, every_value, every_out = (
         lax.all_gather(w_query, "sp", axis=1, tiled=True),
-        lax.all_gather(w_key, "sp", axis=1, tiled=True),
+        jnp.concatenate(lax.all_gather(w_key, "sp"), axis=1),
         lax.all_gather(w_value, "sp", axis=1, tiled=True),
         lax.all_gather(w_out, "sp", axis=2, tiled=True),
     )

time: 784 us -> 785 us (level)
  no operation moved by 1% of the time
where the time goes in v1:
time: 785 us; the launch traced here: 784 us
  waiting for transfers between devices  668 us (85%)
  matrix products  40.9 us (5%)
  local copies, waits for them, and re-layouts  38.7 us (5%)
  other arithmetic  15.1 us (2%)
  between operations  13.8 us (2%)
  starting transfers between devices  7.93 us (1%)
    all_gather x1, waiting for transfers between devices, on_device(): lax.all_gather(w_query, 'sp', axis=1, tiled=True)  150 us
    all_gather x1, waiting for transfers between devices, on_device(): lax.all_gather(w_value, 'sp', axis=1, tiled=True)  143 us
    all_gather x1, waiting for transfers between devices, on_device(): lax.all_gather(w_key, 'sp')  140 us
    all_gather x1, waiting for transfers between devices, on_device(): lax.all_gather(w_out, 'sp', axis=2, tiled=True)  131 us
    psum x2, waiting for transfers between devices, on_device(): lax.psum(jnp.dot(attended, out_weight, preferred_element_type=jnp.float32...  101 us
  transfers between devices with their start and end apart: 10, of which 6 were waited for; matrix products, arithmetic and copies ran while one was open for 7% of the time, Pallas kernels for 0%

profile of v1, /device:TPU:0, one launch (start us, length us, event | category | flops | bytes accessed | tf_op | source)
XLA Modules:
  0.0 784.2 jit_solution(17233687865404392574)
XLA Ops:
  10.5 3.9 fusion.28
  14.4 6.0 copy.29
  21.0 140.3 %all-gather.12.cloned.1.call-done = bf16[8,1024,512]{2,1,0:T(8,128)(2,1)} async-done(((bf16[2,1024,512]{2,1,0:T(8,128)(2,1)}), bf16[8,1024,512]{2,1,0:T(8,128)(2,1)}) %all-gather.12.cloned.1.call-update) | async-done | bytes 8388624 | tf_op jit(solution)/shard_map/all_gather | solution.py:64
  161.3 5.1 fusion.89
  167.7 142.9 %all-gather.6.cloned.1.call-done = bf16[2,4096,512]{2,1,0:T(8,128)(2,1)} async-done(((bf16[2,1024,512]{2,1,0:T(8,128)(2,1)}), bf16[2,4096,512]{2,1,0:T(8,128)(2,1)}) %all-gather.6.cloned.1.call-update) | async-done | bytes 8388624 | tf_op jit(solution)/shard_map/all_gather | solution.py:65
  310.7 3.5 fusion.52
  314.2 1.3 collective-permute-start
  315.5 1.5 collective-permute-start.1
  317.0 150.4 %all-gather.8.cloned.1.call-done = bf16[2,4096,512]{2,1,0:T(8,128)(2,1)} async-done(((bf16[2,1024,512]{2,1,0:T(8,128)(2,1)}), bf16[2,4096,512]{2,1,0:T(8,128)(2,1)}) %all-gather.8.cloned.1.call-update) | async-done | bytes 8388624 | tf_op jit(solution)/shard_map/all_gather | solution.py:63
  467.4 4.2 fusion.53
  472.6 2.4 pad_maximum_fusion
  475.0 4.4 gather_fusion
  479.5 3.3 slice_bitcast_fusion.15
  486.1 130.8 %all-gather.10.cloned.1.call-done = bf16[2,512,4096]{2,1,0:T(8,128)(2,1)} async-done(((bf16[2,512,1024]{2,1,0:T(8,128)(2,1)}), bf16[2,512,4096]{2,1,0:T(8,128)(2,1)}) %all-gather.10.cloned.1.call-update) | async-done | bytes 8388624 | tf_op jit(solution)/shard_map/all_gather | solution.py:66
  616.9 4.8 convolution_convert_fusion.1
  621.8 2.3 fusion.67
  624.1 47.4 %all-reduce.4.cloned.1.call-done = bf16[256,4096]{1,0:T(8,128)(2,1)} async-done(((bf16[256,4096]{1,0:T(8,128)(2,1)}), bf16[256,4096]{1,0:T(8,128)(2,1)}) %all-reduce.4.cloned.1.call-update) | async-done | bytes 2097168 | tf_op jit(solution)/shard_map/psum | solution.py:104
  671.4 2.5 fusion.4
  675.0 1.8 copy-done.5
  678.0 3.6 fusion.54
  681.7 3.4 collective-permute-start.2
  685.1 1.5 collective-permute-start.3
  686.7 3.8 fusion.26
  690.5 5.8 copy.36
  696.3 4.8 fusion.55
  702.1 2.4 pad_maximum_fusion.1
  704.4 4.2 gather_fusion.1
  708.6 3.1 slice_bitcast_fusion.13
  715.3 1.5 slice-done.1
  716.7 2.6 convolution_convert_fusion
  719.4 53.3 %all-reduce.6.cloned.1.call-done = bf16[256,4096]{1,0:T(8,128)(2,1)} async-done(((bf16[256,4096]{1,0:T(8,128)(2,1)}), bf16[256,4096]{1,0:T(8,128)(2,1)}) %all-reduce.6.cloned.1.call-update) | async-done | bytes 2097168 | tf_op jit(solution)/shard_map/psum | solution.py:104
  772.7 4.7 fusion.7
  (64 shorter events, 17.0 us)
Async XLA Ops:
  6.5 2.9 copy-start.8
  6.5 154.7 %all-gather.12.cloned.1.call-start = ((), (), s32[]{:S(2)}) async-start(), calls=%async_computation.5 | async-start | bytes 10485760 | tf_op jit(solution)/shard_map/all_gather | solution.py:64
  7.3 303.4 %all-gather.6.cloned.1.call-start = ((), (), s32[]{:S(2)}) async-start(), calls=%async_computation | async-start | bytes 10485760 | tf_op jit(solution)/shard_map/all_gather | solution.py:65
  8.0 459.4 %all-gather.8.cloned.1.call-start = ((), (), s32[]{:S(2)}) async-start(), calls=%async_computation.1 | async-start | bytes 10485760 | tf_op jit(solution)/shard_map/all_gather | solution.py:63
  8.7 608.2 %all-gather.10.cloned.1.call-start = ((), (), s32[]{:S(2)}) async-start(), calls=%async_computation.2 | async-start | bytes 10485760 | tf_op jit(solution)/shard_map/all_gather | solution.py:66
  9.3 662.1 %all-reduce.4.cloned.1.call-start = ((), (), s32[]{:S(2)}) async-start(), calls=%async_computation.3 | async-start | bytes 4194304 | tf_op jit(solution)/shard_map/psum | solution.py:104
  14.4 6.0 copy-start
  14.4 6.6 copy-start.7
  314.2 158.4 %collective-permute-start = (bf16[4,64,1024]{2,1,0:T(8,128)(2,1)S(1)}, bf16[4,64,1024]{2,1,0:T(8,128)(2,1)S(1)}, u32[]{:S(2)}, u32[]{:S(2)}) collective-permute-start(bf16[4,64,1024]{2,1,0:T(8,128)(2,1)S(1)} %bitcast.158), channel_id=1, source_target_pairs={{0,4},{4,8},{8,12},{1,5},{5,9},{9,13},{2,6},{6,10},{10,14},{3,7},{... | collective-permute-start | bytes 1572872 | tf_op jit(solution)/shard_map/ppermute | solution.py:19
  315.5 157.1 %collective-permute-start.1 = (bf16[4,64,1024]{2,1,0:T(8,128)(2,1)S(1)}, bf16[4,64,1024]{2,1,0:T(8,128)(2,1)}, u32[]{:S(2)}, u32[]{:S(2)}) collective-permute-start(bf16[4,64,1024]{2,1,0:T(8,128)(2,1)S(1)} %bitcast.159), channel_id=1, source_target_pairs={{4,0},{8,4},{12,8},{5,1},{9,5},{13,9},{6,2},{10,6},{14,10},{7,3},{... | collective-permute-start | bytes 1572872 | tf_op jit(solution)/shard_map/ppermute | solution.py:22
  479.5 3.7 copy-start.2
  621.7 151.0 %all-reduce.6.cloned.1.call-start = ((), (), s32[]{:S(2)}) async-start(), calls=%async_computation.4 | async-start | bytes 4194304 | tf_op jit(solution)/shard_map/psum | solution.py:104
  671.4 2.5 copy-start.1
  673.9 2.8 copy-start.5
  674.9 6.7 copy-start.6
  678.0 8.6 %copy-start.4 = (f32[64,64,4,15]{1,3,0,2:T(8,128)S(1)}, f32[64,64,4,15]{1,3,0,2:T(8,128)}, u32[]{:S(2)}) copy-start(f32[64,64,4,15]{1,3,0,2:T(8,128)} %fusion.67) | copy-start | bytes 2949124
  681.7 20.4 %collective-permute-start.2 = (bf16[4,64,1024]{2,1,0:T(8,128)(2,1)S(1)}, bf16[4,64,1024]{2,1,0:T(8,128)(2,1)S(1)}, u32[]{:S(2)}, u32[]{:S(2)}) collective-permute-start(bf16[4,64,1024]{2,1,0:T(8,128)(2,1)S(1)} %bitcast.155), channel_id=1, source_target_pairs={{0,4},{4,8},{8,12},{1,5},{5,9},{9,13},{2,6},{6,10},{10,14},{3,7},{... | collective-permute-start | bytes 1572872 | tf_op jit(solution)/shard_map/ppermute | solution.py:19
  685.1 17.0 %collective-permute-start.3 = (bf16[4,64,1024]{2,1,0:T(8,128)(2,1)S(1)}, bf16[4,64,1024]{2,1,0:T(8,128)(2,1)}, u32[]{:S(2)}, u32[]{:S(2)}) collective-permute-start(bf16[4,64,1024]{2,1,0:T(8,128)(2,1)S(1)} %bitcast.156), channel_id=1, source_target_pairs={{4,0},{8,4},{12,8},{5,1},{9,5},{13,9},{6,2},{10,6},{14,10},{7,3},{... | collective-permute-start | bytes 1572872 | tf_op jit(solution)/shard_map/ppermute | solution.py:22
  708.6 3.4 copy-start.3
  713.1 2.2 slice-start
  713.8 2.9 slice-start.1
Sparse Core Ops, SparseCore 0:
  8.9 152.3 all-gather.11
  162.8 147.7 all-gather.5
  312.2 155.1 all-gather.7
  468.8 148.0 all-gather.9
  621.8 49.5 all-reduce.3
  719.5 53.1 all-reduce.5
